TPU v7x, 32 devices: a whole 2x2x4 slice. The times are simulated.
32 devices in a mesh: kv: 8 (over z, x), tp: 4 (over y, core).
Axes of the slice: x: 2, y: 2, z: 4, core: 2. Of those that a mesh axis runs over, the one named last changes fastest.
Arguments:
- tokens: bfloat16 [96, 2048], P('tp', 'kv'), may hold values from -10.5 to 10.5
- norm_gain: float32 [2048], P('kv'), may hold values from 0.1 to 1.9
- w_query: bfloat16 [2048, 2048], P('kv', 'tp'), may hold values from -0.125 to 0.125
- w_forget: bfloat16 [2048, 2048], P('kv', 'tp'), may hold values from -0.125 to 0.125
- w_input: bfloat16 [2048, 2048], P('kv', 'tp'), may hold values from -0.125 to 0.125
- w_gate: bfloat16 [2048, 2048], P('kv', 'tp'), may hold values from -0.125 to 0.125
- lower_bound: float32 [2048], P('tp'), may hold values from 0 to 0.9
- head_gain: float32 [16, 128], P('tp'), may hold values from 0.1 to 1.9
- recur_state: float32 [96, 16, 128, 128], P('kv', 'tp'), may hold values from -3 to 3
- w_out: bfloat16 [2048, 2048], P('tp', 'kv'), may hold values from -0.125 to 0.125
- mixer_gain: float32 [2048], P('kv'), may hold values from 0.1 to 1.9
- w_up: bfloat16 [2048, 8192], P('kv', 'tp'), may hold values from -0.125 to 0.125
- w_down: bfloat16 [8192, 2048], P('tp', 'kv'), may hold values from -0.0625 to 0.0625
Outputs:
- next_tokens: bfloat16 [96, 2048], P('tp', 'kv')
- next_state: float32 [96, 16, 128, 128], P('kv', 'tp')
All inputs are finite; a program needn't handle non-finite values.
Results may differ from a plain program's by a relative error of at most 0.03.
Values may be sent and summed in bfloat16 or wider, within the bound.
A program may use at most 64 MiB of HBM per device.

v0:
```python
import functools

import jax
import jax.numpy as jnp
from jax import lax
from jax.experimental import pallas as pl
from jax.experimental.pallas import tpu as pltpu
from jax.sharding import PartitionSpec as P

NORM_EPS = 1e-05
F32 = jnp.float32
BF16 = jnp.bfloat16


def round_up(value, step):
    return (value + step - 1) // step * step


def remote(src, dst, send_sem, recv_sem, axis, peer):
    return pltpu.make_async_remote_copy(
        src_ref=src,
        dst_ref=dst,
        send_sem=send_sem,
        recv_sem=recv_sem,
        device_id={axis: peer},
        device_id_type=pl.DeviceIdType.MESH,
    )


def kernel(
    n_kv,
    n_tp,
    tok_hbm,
    gain_hbm,
    wq_hbm,
    wf_hbm,
    wi_hbm,
    wg_hbm,
    bound_hbm,
    hgain_hbm,
    state_hbm,
    wo_hbm,
    mgain_hbm,
    wu_hbm,
    wd_hbm,
    out_ref,
    ns_ref,
    gain_ref,
    bound_ref,
    hgain_ref,
    mgain_ref,
    w_in,
    wo,
    wu,
    wd,
    state,
    state_bf,
    tokbuf,
    send2,
    pair2,
    out2,
    recv2,
    sq_send,
    sq_recv,
    mix_send,
    mix_recv,
    send4,
    recv4,
    mixed_buf,
    send5,
    pair5,
    out5,
    recv5,
    sq5_send,
    sq5_recv,
    hid_send,
    hid_recv,
    send7,
    recv7,
    load_sem,
    tp_send_sem,
    tp_recv_sem,
    kv_send_sem,
    kv_recv_sem,
):
    kv = lax.axis_index("kv")
    tp = lax.axis_index("tp")
    row_block, feats = tok_hbm.shape
    rows = row_block * n_tp
    own, heads, key, val = state_hbm.shape
    span = heads * key
    pad_rows = sq_send.shape[1]
    chunk = send5.shape[2]
    width = feats * n_kv
    half_rows = rows // 2
    half_blocks = n_tp // 2
    n_far = n_kv // 2
    far, near = kv // 2, lax.rem(kv, 2)
    partner = 2 * far + 1 - near
    if n_far == 4:
        far_peers = [3 - far, lax.rem(far + 2, 4), far + 1 - 2 * lax.rem(far, 2)]
    else:
        far_peers = [lax.rem(far + off, n_far) for off in range(1, n_far)]

    small = [
        pltpu.make_async_copy(tok_hbm, tokbuf.at[tp], load_sem.at[8]),
        pltpu.make_async_copy(gain_hbm, gain_ref, load_sem.at[9]),
        pltpu.make_async_copy(bound_hbm, bound_ref, load_sem.at[10]),
        pltpu.make_async_copy(hgain_hbm, hgain_ref, load_sem.at[11]),
        pltpu.make_async_copy(mgain_hbm, mgain_ref, load_sem.at[12]),
    ]
    for copy in small:
        copy.start()
    loads = []
    for i, src in enumerate((wq_hbm, wf_hbm, wi_hbm, wg_hbm)):
        loads.append(pltpu.make_async_copy(src, w_in.at[i], load_sem.at[i]))
    loads.append(pltpu.make_async_copy(state_hbm, state, load_sem.at[4]))
    loads.append(pltpu.make_async_copy(wo_hbm, wo, load_sem.at[5]))
    loads.append(pltpu.make_async_copy(wu_hbm, wu, load_sem.at[6]))
    loads.append(pltpu.make_async_copy(wd_hbm, wd, load_sem.at[7]))
    for copy in loads:
        copy.start()

    def kv_peer(off):
        return lax.rem(kv + off, n_kv)

    def tp_peer(off):
        return lax.rem(tp + off, n_tp)

    barrier = pltpu.get_barrier_semaphore()
    for off in range(1, n_kv):
        pl.semaphore_signal(
            barrier, inc=1, device_id={"kv": kv_peer(off)}, device_id_type=pl.DeviceIdType.MESH
        )
    for off in range(1, n_tp):
        pl.semaphore_signal(
            barrier, inc=1, device_id={"tp": tp_peer(off)}, device_id_type=pl.DeviceIdType.MESH
        )
    pl.semaphore_wait(barrier, n_kv + n_tp - 2)

    def tp_copy(phase, src, dst_of, peer, slot):
        return remote(
            src,
            dst_of.at[slot],
            tp_send_sem.at[phase, peer],
            tp_recv_sem.at[phase, slot],
            "tp",
            peer,
        )

    def kv_copy(phase, src, dst_of, peer, slot):
        return remote(
            src,
            dst_of.at[slot],
            kv_send_sem.at[phase, peer],
            kv_recv_sem.at[phase, slot],
            "kv",
            peer,
        )

    sent = []

    def send(copy):
        copy.start()
        sent.append(copy)

    def block_copy(phase, src, dst_of, peer, slot, index):
        return remote(
            src,
            dst_of.at[slot],
            kv_send_sem.at[phase, index],
            kv_recv_sem.at[phase, slot],
            "kv",
            peer,
        )

    def pair_send(phase, source, pair, half, at):
        src = source.at[half * n_kv + 2 * at + 1 - near]
        slot = half * n_far + at
        send(block_copy(phase, src, pair, partner, slot, slot))

    def pair_wait(phase, pair, half, at):
        slot = half * n_far + at
        block_copy(phase, pair.at[slot], pair, partner, slot, slot).wait_recv()
        return pair[slot].astype(F32)

    def far_send(phase, out, received, half, at):
        src = out.at[half * n_far + at]
        slot = half * n_far + far
        send(block_copy(phase, src, received, 2 * at + near, slot, half * n_far + at))

    def far_wait(phase, received, half, at):
        slot = half * n_far + at
        block_copy(phase, received.at[slot], received, 2 * at + near, slot, slot).wait_recv()
        return received[slot].astype(F32)

    for copy in small:
        copy.wait()
    for off in range(1, n_tp):
        copy = tp_copy(0, tokbuf.at[tp], tokbuf, tp_peer(off), tp)
        copy.start()
        sent.append(copy)
    for off in range(1, n_tp):
        src = tp_peer(off)
        tp_copy(0, tokbuf.at[src], tokbuf, src, src).wait_recv()
    tokens = jnp.concatenate([tokbuf[t].astype(F32) for t in range(n_tp)], axis=0)

    row_at = lax.broadcasted_iota(jnp.int32, (rows, pad_rows), 0)
    col_at = lax.broadcasted_iota(jnp.int32, (rows, pad_rows), 1)
    diagonal = row_at == col_at

    def as_row(column):
        return jnp.sum(jnp.where(diagonal, column, 0.0), axis=0, keepdims=True)

    normed = (tokens * gain_ref[...]).astype(BF16)
    sq_send[...] = as_row(jnp.sum(tokens * tokens, axis=1, keepdims=True))
    sq_recv[kv] = sq_send[...]
    for half in range(2):
        parts = []
        for i in (2 * half, 2 * half + 1):
            loads[i].wait()
            parts.append(jnp.dot(normed, w_in[i], preferred_element_type=F32))
        for d in range(n_kv):
            send2[half * n_kv + d] = jnp.concatenate(
                [part[d * own : (d + 1) * own] for part in parts], axis=0
            ).astype(BF16)
        for at in far_peers + [far]:
            pair_send(1, send2, pair2, half, at)
    for off in range(1, n_kv):
        send(kv_copy(0, sq_send, sq_recv, kv_peer(off), kv))
    for half in range(2):
        for at in far_peers:
            own_part = send2[half * n_kv + 2 * at + near].astype(F32)
            out2[half * n_far + at] = (own_part + pair_wait(1, pair2, half, at)).astype(BF16)
            far_send(2, out2, recv2, half, at)
    totals = []
    for half in range(2):
        totals.append(send2[half * n_kv + kv].astype(F32) + pair_wait(1, pair2, half, far))
    loads[4].wait()
    for s in range(own):
        for h in range(heads):
            state_bf[h, :, s * val : (s + 1) * val] = state[s, h].astype(BF16)

    for half in range(2):
        for at in far_peers:
            totals[half] = totals[half] + far_wait(2, recv2, half, at)
    for off in range(1, n_kv):
        src = kv_peer(n_kv - off)
        kv_copy(0, sq_send, sq_recv, src, src).wait_recv()
    sq_total = sq_recv[0]
    for d in range(1, n_kv):
        sq_total = sq_total + sq_recv[d]
    own_at = lax.broadcasted_iota(jnp.int32, (own, pad_rows), 0) + kv * own
    lane_at = lax.broadcasted_iota(jnp.int32, (own, pad_rows), 1)
    own_sq = jnp.sum(jnp.where(own_at == lane_at, sq_total, 0.0), axis=1, keepdims=True)
    scale = lax.rsqrt(own_sq / width + NORM_EPS)
    queries = totals[0][:own] * scale
    forget_raw = totals[0][own:] * scale
    values_in = totals[1][:own] * scale
    gate = totals[1][own:] * scale
    bound = bound_ref[...]
    forget = bound + (1.0 - bound) * jax.nn.sigmoid(forget_raw)
    decayed = queries * forget
    fresh = queries - decayed
    decayed = decayed.astype(BF16)
    seq_at = lax.broadcasted_iota(jnp.int32, (own, val), 0)
    mixture = []
    for h in range(heads):
        cols = slice(h * key, (h + 1) * key)
        vals = slice(h * val, (h + 1) * val)
        wide = jnp.dot(decayed[:, cols], state_bf[h], preferred_element_type=F32)
        read = jnp.sum(fresh[:, cols], axis=1, keepdims=True) * values_in[:, vals]
        for s in range(own):
            read = read + jnp.where(seq_at == s, wide[:, s * val : (s + 1) * val], 0.0)
        mean = jnp.mean(read * read, axis=1, keepdims=True)
        read = read * lax.rsqrt(mean + NORM_EPS) * hgain_ref[h : h + 1]
        mixture.append(read * jax.nn.silu(gate[:, vals]))
    mix_send[...] = jnp.concatenate(mixture, axis=0).astype(BF16)
    for off in range(1, n_kv):
        copy = kv_copy(3, mix_send, mix_recv, kv_peer(off), kv)
        copy.start()
        sent.append(copy)
    mix_recv[kv] = mix_send[...]

    for h in range(heads):
        cols = slice(h * key, (h + 1) * key)
        vals = slice(h * val, (h + 1) * val)
        fill = jnp.zeros((round_up(own, 128) - own, key), F32)
        turned = jnp.concatenate([forget[:, cols], fill], axis=0).T
        for s in range(own):
            fresh_row = values_in[s : s + 1, vals]
            ns_ref[s, h] = fresh_row + turned[:, s : s + 1] * (state[s, h] - fresh_row)

    loads[5].wait()
    for off in range(1, n_kv):
        src = kv_peer(n_kv - off)
        kv_copy(3, mix_send, mix_recv, src, src).wait_recv()
    blocks = [mix_recv[d].astype(F32) for d in range(n_kv)]
    gathered = jnp.concatenate(
        [
            jnp.concatenate([block[h * own : (h + 1) * own] for block in blocks], axis=0)
            for h in range(heads)
        ],
        axis=1,
    ).astype(BF16)
    for half in range(2):
        here = gathered[half * half_rows : (half + 1) * half_rows]
        send4[half] = jnp.dot(here, wo[...], preferred_element_type=F32).astype(BF16)
        for off in range(1, n_tp):
            send(tp_copy(1 + half, send4.at[half], recv4.at[half], tp_peer(off), tp))
        recv4[half, tp] = send4[half]
    loads[6].wait()
    aligned = chunk % 128 == 0

    def up(half, normed, peer):
        if not aligned:
            return send5[half * n_kv + peer].astype(F32)
        columns = pl.ds(pl.multiple_of(peer * chunk, 128), chunk)
        return jnp.dot(normed, wu[:, columns], preferred_element_type=F32)

    normed_halves = []
    squares = 0.0
    for half in range(2):
        for off in range(1, n_tp):
            src = tp_peer(off)
            tp_copy(1 + half, send4.at[half], recv4.at[half], src, src).wait_recv()
        attn = recv4[half, 0].astype(F32)
        for t in range(1, n_tp):
            attn = attn + recv4[half, t].astype(F32)
        blocks = range(half * half_blocks, (half + 1) * half_blocks)
        tokens = jnp.concatenate([tokbuf[t].astype(F32) for t in blocks], axis=0)
        mixed = (tokens + attn).astype(BF16).astype(F32)
        for i, t in enumerate(blocks):
            mixed_buf[t] = mixed[i * row_block : (i + 1) * row_block]
        normed = (mixed * mgain_ref[...]).astype(BF16)
        normed_halves.append(normed)
        if not aligned:
            hidden_all = jnp.dot(normed, wu[...], preferred_element_type=F32).astype(BF16)
            for c in range(n_kv):
                send5[half * n_kv + c] = hidden_all[:, c * chunk : (c + 1) * chunk]
        for at in far_peers + [far]:
            peer = 2 * at + 1 - near
            if aligned:
                send5[half * n_kv + peer] = up(half, normed, peer).astype(BF16)
            pair_send(5, send5, pair5, half, at)
        half_at = diagonal[half * half_rows : (half + 1) * half_rows]
        column = jnp.sum(mixed * mixed, axis=1, keepdims=True)
        squares = squares + jnp.sum(jnp.where(half_at, column, 0.0), axis=0, keepdims=True)
    sq5_send[...] = squares
    sq5_recv[kv] = squares
    for off in range(1, n_kv):
        send(kv_copy(4, sq5_send, sq5_recv, kv_peer(off), kv))
    for half in range(2):
        for at in far_peers:
            own_part = up(half, normed_halves[half], 2 * at + near)
            out5[half * n_far + at] = (own_part + pair_wait(5, pair5, half, at)).astype(BF16)
            far_send(6, out5, recv5, half, at)
    for off in range(1, n_kv):
        src = kv_peer(n_kv - off)
        kv_copy(4, sq5_send, sq5_recv, src, src).wait_recv()
    sq_total = sq5_recv[0]
    for d in range(1, n_kv):
        sq_total = sq_total + sq5_recv[d]
    row_sq = jnp.sum(jnp.where(diagonal, sq_total, 0.0), axis=1, keepdims=True)
    row_scale = lax.rsqrt(row_sq / width + NORM_EPS)
    for half in range(2):
        total = up(half, normed_halves[half], kv) + pair_wait(5, pair5, half, far)
        for at in far_peers:
            total = total + far_wait(6, recv5, half, at)
        scale = row_scale[half * half_rows : (half + 1) * half_rows]
        hidden = jnp.maximum(total * scale, 0.0)
        hid_send[half] = (hidden * hidden).astype(BF16)
        slot = half * n_kv + kv
        for at in far_peers:
            peer = 2 * at + near
            send(block_copy(7, hid_send.at[half], hid_recv, peer, slot, half * n_far + at))
        send(block_copy(7, hid_send.at[half], hid_recv, partner, slot, half * n_far + far))
    loads[7].wait()

    def down(source, block):
        at = pl.ds(pl.multiple_of(source * chunk, chunk), chunk)
        return jnp.dot(block, wd[at, :], preferred_element_type=F32)

    def hid_wait(half, src):
        slot = half * n_kv + src
        block_copy(7, hid_send.at[half], hid_recv, partner, slot, half * n_far + far).wait_recv()

    sums = []
    for half in range(2):
        total = down(kv, hid_send[half])
        hid_wait(half, partner)
        total = total + down(partner, hid_recv[half * n_kv + partner])
        for at in reversed(far_peers):
            src = 2 * at + near
            slot = half * n_kv + src
            hid_wait(half, src)
            send(
                remote(
                    hid_recv.at[slot],
                    hid_recv.at[slot],
                    kv_send_sem.at[8, half * n_far + at],
                    kv_recv_sem.at[7, slot],
                    "kv",
                    partner,
                )
            )
            total = total + down(src, hid_recv[slot])
        sums.append(total)
    for half in range(2):
        total = sums[half]
        for at in reversed(far_peers):
            src = 2 * at + 1 - near
            hid_wait(half, src)
            total = total + down(src, hid_recv[half * n_kv + src])
        for i in range(half_blocks):
            t = half * half_blocks + i
            send7[t] = total[i * row_block : (i + 1) * row_block].astype(BF16)

            @pl.when(t != tp)
            def _():
                tp_copy(3, send7.at[t], recv7, t, tp).start()

    recv7[tp] = send7[tp]
    for off in range(1, n_tp):
        src = tp_peer(off)
        tp_copy(3, recv7.at[src], recv7, src, src).wait_recv()
        tp_copy(3, send7.at[src], recv7, src, tp).wait_send()
    down_out = recv7[0].astype(F32)
    for t in range(1, n_tp):
        down_out = down_out + recv7[t].astype(F32)
    out_ref[...] = (mixed_buf[tp] + down_out).astype(BF16)
    for copy in sent:
        copy.wait_send()


def solution(mesh):
    n_kv, n_tp = mesh.shape["kv"], mesh.shape["tp"]

    def body(
        tokens,
        norm_gain,
        w_query,
        w_forget,
        w_input,
        w_gate,
        lower_bound,
        head_gain,
        recur_state,
        w_out,
        mixer_gain,
        w_up,
        w_down,
    ):
        row_block, feats = tokens.shape
        rows = row_block * n_tp
        own, heads, key, val = recur_state.shape
        span = w_query.shape[1]
        units = w_up.shape[1]
        chunk = units // n_kv
        pad_rows = round_up(rows, 128)
        kept = recur_state.size * 4 + round_up(row_block, 16) * round_up(feats, 128) * 2
        grant = 67043328 - kept - 16384
        vmem = pl.BlockSpec(memory_space=pltpu.VMEM)
        hbm = pl.BlockSpec(memory_space=pltpu.HBM)
        next_tokens, next_state = pl.pallas_call(
            functools.partial(kernel, n_kv, n_tp),
            out_shape=(
                pltpu.VMEM(tokens.shape, BF16),
                pltpu.VMEM(recur_state.shape, F32),
            ),
            in_specs=[hbm] * 13,
            out_specs=(vmem, vmem),
            scratch_shapes=[
                pltpu.VMEM((1, feats), F32),
                pltpu.VMEM((1, span), F32),
                pltpu.VMEM(head_gain.shape, F32),
                pltpu.VMEM((1, feats), F32),
                pltpu.VMEM((4, feats, span), BF16),
                pltpu.VMEM(w_out.shape, BF16),
                pltpu.VMEM(w_up.shape, BF16),
                pltpu.VMEM(w_down.shape, BF16),
                pltpu.VMEM(recur_state.shape, F32),
                pltpu.VMEM((heads, key, own * val), BF16),
                pltpu.VMEM((n_tp, row_block, feats), BF16),
                pltpu.VMEM((2 * n_kv, 2 * own, span), BF16),
                pltpu.VMEM((n_kv, 2 * own, span), BF16),
                pltpu.VMEM((n_kv, 2 * own, span), BF16),
                pltpu.VMEM((n_kv, 2 * own, span), BF16),
                pltpu.VMEM((1, pad_rows), F32),
                pltpu.VMEM((n_kv, 1, pad_rows), F32),
                pltpu.VMEM((heads * own, val), BF16),
                pltpu.VMEM((n_kv, heads * own, val), BF16),
                pltpu.VMEM((2, rows // 2, feats), BF16),
                pltpu.VMEM((2, n_tp, rows // 2, feats), BF16),
                pltpu.VMEM((n_tp, row_block, feats), F32),
                pltpu.VMEM((2 * n_kv, rows // 2, chunk), BF16),
                pltpu.VMEM((n_kv, rows // 2, chunk), BF16),
                pltpu.VMEM((n_kv, rows // 2, chunk), BF16),
                pltpu.VMEM((n_kv, rows // 2, chunk), BF16),
                pltpu.VMEM((1, pad_rows), F32),
                pltpu.VMEM((n_kv, 1, pad_rows), F32),
                pltpu.VMEM((2, rows // 2, chunk), BF16),
                pltpu.VMEM((2 * n_kv, rows // 2, chunk), BF16),
                pltpu.VMEM((n_tp, row_block, feats), BF16),
                pltpu.VMEM((n_tp, row_block, feats), BF16),
                pltpu.SemaphoreType.DMA((13,)),
                pltpu.SemaphoreType.DMA((4, n_tp)),
                pltpu.SemaphoreType.DMA((4, n_tp)),
                pltpu.SemaphoreType.DMA((9, 2 * n_kv)),
                pltpu.SemaphoreType.DMA((9, 2 * n_kv)),
            ],
            compiler_params=pltpu.CompilerParams(collective_id=0, has_side_effects=True, vmem_limit_bytes=grant),
        )(
            tokens,
            norm_gain.reshape(1, feats),
            w_query,
            w_forget,
            w_input,
            w_gate,
            lower_bound.reshape(1, span),
            head_gain,
            recur_state,
            w_out,
            mixer_gain.reshape(1, feats),
            w_up,
            w_down,
        )
        return next_tokens, next_state

    in_specs = (
        P("tp", "kv"),
        P("kv"),
        P("kv", "tp"),
        P("kv", "tp"),
        P("kv", "tp"),
        P("kv", "tp"),
        P("tp"),
        P("tp", None),
        P("kv", "tp", None, None),
        P("tp", "kv"),
        P("kv"),
        P("kv", "tp"),
        P("tp", "kv"),
    )
    out_specs = (P("tp", "kv"), P("kv", "tp", None, None))
    return jax.shard_map(body, mesh=mesh, in_specs=in_specs, out_specs=out_specs, check_vma=False)
```

profile of v0, /device:TPU:0, one launch (start us, length us, event | category | flops | bytes accessed | tf_op | source)
XLA Modules:
  0.0 50.9 jit_solution(14810932432746166292)
XLA Ops:
  0.6 48.0 %shard_map.140 = (bf16[24,256]{1,0:T(8,128)(2,1)S(1)}, f32[12,4,128,128]{3,2,1,0:T(8,128)S(1)}) custom-call(bf16[24,256]{1,0:T(8,128)(2,1)} %tok_hbm.1, f32[1,256]{1,0:T(1,128)} %bitcast.4, bf16[256,512]{1,0:T(8,128)(2,1)} %wq_hbm.1, bf16[256,512]{1,0:T(8,128)(2,1)} %wf_hbm.1, bf16[256,512]{1,0:T(8,128)(2,1)} %wi_hbm.1, bf16[256,512]{1,0:T(8,128)(2,1)} %wg_hbm.1, ...), custom_call_target="tpu_custom_call" | custom-call | tf_op jit(solution)/shard_map/pallas_call | solution.py:465
  48.7 0.6 %copy.17 = bf16[24,256]{1,0:T(8,128)(2,1)} copy(bf16[24,256]{1,0:T(8,128)(2,1)S(1)} %get-tuple-element.2) | data formatting | bytes 24576
  49.3 1.7 %copy.18 = f32[12,4,128,128]{3,2,1,0:T(8,128)} copy(f32[12,4,128,128]{3,2,1,0:T(8,128)S(1)} %get-tuple-element.3) | data formatting | bytes 6291456
where the time goes:
time: 51.1 us; the launch traced here: 50.9 us
  Pallas kernels  48 us (94%)
  local copies, waits for them, and re-layouts  2.27 us (4%)
  between operations  0.64 us (1%)
    pallas_call x1, Pallas kernels, body(): pl.pallas_call(functools.partial(kernel, n_kv, n_tp), out_shape=(pltpu.VM...  48 us
    unnamed x2, local copies, waits for them, and re-layouts  2.27 us

commit v1 on v0

--- a/solution.py
+++ b/solution.py
@@ -78,10 +78,13 @@
     send7,
     recv7,
     load_sem,
-    tp_send_sem,
+    send_sem,
     tp_recv_sem,
-    kv_send_sem,
-    kv_recv_sem,
+    sq_recv_sem,
+    mix_recv_sem,
+    pair_recv_sem,
+    far_recv_sem,
+    hid_recv_sem,
 ):
     kv = lax.axis_index("kv")
     tp = lax.axis_index("tp")
@@ -138,71 +141,37 @@
         )
     pl.semaphore_wait(barrier, n_kv + n_tp - 2)
 
-    def tp_copy(phase, src, dst_of, peer, slot):
-        return remote(
-            src,
-            dst_of.at[slot],
-            tp_send_sem.at[phase, peer],
-            tp_recv_sem.at[phase, slot],
-            "tp",
-            peer,
-        )
-
-    def kv_copy(phase, src, dst_of, peer, slot):
-        return remote(
-            src,
-            dst_of.at[slot],
-            kv_send_sem.at[phase, peer],
-            kv_recv_sem.at[phase, slot],
-            "kv",
-            peer,
-        )
-
-    sent = []
-
-    def send(copy):
-        copy.start()
-        sent.append(copy)
-
-    def block_copy(phase, src, dst_of, peer, slot, index):
-        return remote(
-            src,
-            dst_of.at[slot],
-            kv_send_sem.at[phase, index],
-            kv_recv_sem.at[phase, slot],
-            "kv",
-            peer,
-        )
+    def tp_copy(phase, send_at, src, dst, peer):
+        return remote(src, dst, send_sem.at[send_at], tp_recv_sem.at[phase], "tp", peer)
+
+    def kv_copy(send_at, src, dst, recv_sem, peer):
+        return remote(src, dst, send_sem.at[send_at], recv_sem, "kv", peer)
 
     def pair_send(phase, source, pair, half, at):
         src = source.at[half * n_kv + 2 * at + 1 - near]
         slot = half * n_far + at
-        send(block_copy(phase, src, pair, partner, slot, slot))
+        kv_copy(4 * phase + 4, src, pair.at[slot], pair_recv_sem.at[phase, slot], partner).start()
 
     def pair_wait(phase, pair, half, at):
         slot = half * n_far + at
-        block_copy(phase, pair.at[slot], pair, partner, slot, slot).wait_recv()
+        kv_copy(0, pair.at[slot], pair.at[slot], pair_recv_sem.at[phase, slot], partner).wait_recv()
         return pair[slot].astype(F32)
 
     def far_send(phase, out, received, half, at):
         src = out.at[half * n_far + at]
-        slot = half * n_far + far
-        send(block_copy(phase, src, received, 2 * at + near, slot, half * n_far + at))
-
-    def far_wait(phase, received, half, at):
-        slot = half * n_far + at
-        block_copy(phase, received.at[slot], received, 2 * at + near, slot, slot).wait_recv()
-        return received[slot].astype(F32)
+        dst = received.at[half * n_far + far]
+        kv_copy(4 * phase + 5, src, dst, far_recv_sem.at[2 * phase + half], 2 * at + near).start()
+
+    def far_wait(phase, received, half):
+        block = received.at[pl.ds(half * n_far, n_far - 1)]
+        kv_copy(0, block, block, far_recv_sem.at[2 * phase + half], partner).wait_recv()
 
     for copy in small:
         copy.wait()
+    others = pl.ds(0, n_tp - 1)
     for off in range(1, n_tp):
-        copy = tp_copy(0, tokbuf.at[tp], tokbuf, tp_peer(off), tp)
-        copy.start()
-        sent.append(copy)
-    for off in range(1, n_tp):
-        src = tp_peer(off)
-        tp_copy(0, tokbuf.at[src], tokbuf, src, src).wait_recv()
+        tp_copy(0, 0, tokbuf.at[tp], tokbuf.at[tp], tp_peer(off)).start()
+    tp_copy(0, 0, tokbuf.at[others], tokbuf.at[others], tp_peer(1)).wait_recv()
     tokens = jnp.concatenate([tokbuf[t].astype(F32) for t in range(n_tp)], axis=0)
 
     row_at = lax.broadcasted_iota(jnp.int32, (rows, pad_rows), 0)
@@ -225,28 +194,28 @@
                 [part[d * own : (d + 1) * own] for part in parts], axis=0
             ).astype(BF16)
         for at in far_peers + [far]:
-            pair_send(1, send2, pair2, half, at)
+            pair_send(0, send2, pair2, half, at)
     for off in range(1, n_kv):
-        send(kv_copy(0, sq_send, sq_recv, kv_peer(off), kv))
+        kv_copy(1, sq_send, sq_recv.at[kv], sq_recv_sem.at[0], kv_peer(off)).start()
     for half in range(2):
         for at in far_peers:
             own_part = send2[half * n_kv + 2 * at + near].astype(F32)
-            out2[half * n_far + at] = (own_part + pair_wait(1, pair2, half, at)).astype(BF16)
-            far_send(2, out2, recv2, half, at)
+            out2[half * n_far + at] = (own_part + pair_wait(0, pair2, half, at)).astype(BF16)
+            far_send(0, out2, recv2, half, at)
     totals = []
     for half in range(2):
-        totals.append(send2[half * n_kv + kv].astype(F32) + pair_wait(1, pair2, half, far))
+        totals.append(send2[half * n_kv + kv].astype(F32) + pair_wait(0, pair2, half, far))
     loads[4].wait()
     for s in range(own):
         for h in range(heads):
             state_bf[h, :, s * val : (s + 1) * val] = state[s, h].astype(BF16)
 
     for half in range(2):
+        far_wait(0, recv2, half)
         for at in far_peers:
-            totals[half] = totals[half] + far_wait(2, recv2, half, at)
-    for off in range(1, n_kv):
-        src = kv_peer(n_kv - off)
-        kv_copy(0, sq_send, sq_recv, src, src).wait_recv()
+            totals[half] = totals[half] + recv2[half * n_far + at].astype(F32)
+    kv_others = pl.ds(0, n_kv - 1)
+    kv_copy(1, sq_recv.at[kv_others], sq_recv.at[kv_others], sq_recv_sem.at[0], partner).wait_recv()
     sq_total = sq_recv[0]
     for d in range(1, n_kv):
         sq_total = sq_total + sq_recv[d]
@@ -277,9 +246,7 @@
         mixture.append(read * jax.nn.silu(gate[:, vals]))
     mix_send[...] = jnp.concatenate(mixture, axis=0).astype(BF16)
     for off in range(1, n_kv):
-        copy = kv_copy(3, mix_send, mix_recv, kv_peer(off), kv)
-        copy.start()
-        sent.append(copy)
+        kv_copy(2, mix_send, mix_recv.at[kv], mix_recv_sem.at[0], kv_peer(off)).start()
     mix_recv[kv] = mix_send[...]
 
     for h in range(heads):
@@ -292,9 +259,7 @@
             ns_ref[s, h] = fresh_row + turned[:, s : s + 1] * (state[s, h] - fresh_row)
 
     loads[5].wait()
-    for off in range(1, n_kv):
-        src = kv_peer(n_kv - off)
-        kv_copy(3, mix_send, mix_recv, src, src).wait_recv()
+    kv_copy(2, mix_recv.at[kv_others], mix_recv.at[kv_others], mix_recv_sem.at[0], partner).wait_recv()
     blocks = [mix_recv[d].astype(F32) for d in range(n_kv)]
     gathered = jnp.concatenate(
         [
@@ -307,8 +272,8 @@
         here = gathered[half * half_rows : (half + 1) * half_rows]
         send4[half] = jnp.dot(here, wo[...], preferred_element_type=F32).astype(BF16)
         for off in range(1, n_tp):
-            send(tp_copy(1 + half, send4.at[half], recv4.at[half], tp_peer(off), tp))
-        recv4[half, tp] = send4[half]
+            tp_copy(1 + half, 3, send4.at[half], recv4.at[half * n_tp + tp], tp_peer(off)).start()
+        recv4[half * n_tp + tp] = send4[half]
     loads[6].wait()
     aligned = chunk % 128 == 0
 
@@ -321,12 +286,11 @@
     normed_halves = []
     squares = 0.0
     for half in range(2):
-        for off in range(1, n_tp):
-            src = tp_peer(off)
-            tp_copy(1 + half, send4.at[half], recv4.at[half], src, src).wait_recv()
-        attn = recv4[half, 0].astype(F32)
+        block = recv4.at[pl.ds(half * n_tp, n_tp - 1)]
+        tp_copy(1 + half, 3, block, block, tp_peer(1)).wait_recv()
+        attn = recv4[half * n_tp].astype(F32)
         for t in range(1, n_tp):
-            attn = attn + recv4[half, t].astype(F32)
+            attn = attn + recv4[half * n_tp + t].astype(F32)
         blocks = range(half * half_blocks, (half + 1) * half_blocks)
         tokens = jnp.concatenate([tokbuf[t].astype(F32) for t in blocks], axis=0)
         mixed = (tokens + attn).astype(BF16).astype(F32)
@@ -342,39 +306,36 @@
             peer = 2 * at + 1 - near
             if aligned:
                 send5[half * n_kv + peer] = up(half, normed, peer).astype(BF16)
-            pair_send(5, send5, pair5, half, at)
+            pair_send(1, send5, pair5, half, at)
         half_at = diagonal[half * half_rows : (half + 1) * half_rows]
         column = jnp.sum(mixed * mixed, axis=1, keepdims=True)
         squares = squares + jnp.sum(jnp.where(half_at, column, 0.0), axis=0, keepdims=True)
     sq5_send[...] = squares
     sq5_recv[kv] = squares
     for off in range(1, n_kv):
-        send(kv_copy(4, sq5_send, sq5_recv, kv_peer(off), kv))
+        kv_copy(6, sq5_send, sq5_recv.at[kv], sq_recv_sem.at[1], kv_peer(off)).start()
     for half in range(2):
         for at in far_peers:
             own_part = up(half, normed_halves[half], 2 * at + near)
-            out5[half * n_far + at] = (own_part + pair_wait(5, pair5, half, at)).astype(BF16)
-            far_send(6, out5, recv5, half, at)
-    for off in range(1, n_kv):
-        src = kv_peer(n_kv - off)
-        kv_copy(4, sq5_send, sq5_recv, src, src).wait_recv()
+            out5[half * n_far + at] = (own_part + pair_wait(1, pair5, half, at)).astype(BF16)
+            far_send(1, out5, recv5, half, at)
+    kv_copy(6, sq5_recv.at[kv_others], sq5_recv.at[kv_others], sq_recv_sem.at[1], partner).wait_recv()
     sq_total = sq5_recv[0]
     for d in range(1, n_kv):
         sq_total = sq_total + sq5_recv[d]
     row_sq = jnp.sum(jnp.where(diagonal, sq_total, 0.0), axis=1, keepdims=True)
     row_scale = lax.rsqrt(row_sq / width + NORM_EPS)
     for half in range(2):
-        total = up(half, normed_halves[half], kv) + pair_wait(5, pair5, half, far)
+        total = up(half, normed_halves[half], kv) + pair_wait(1, pair5, half, far)
+        far_wait(1, recv5, half)
         for at in far_peers:
-            total = total + far_wait(6, recv5, half, at)
+            total = total + recv5[half * n_far + at].astype(F32)
         scale = row_scale[half * half_rows : (half + 1) * half_rows]
         hidden = jnp.maximum(total * scale, 0.0)
         hid_send[half] = (hidden * hidden).astype(BF16)
         slot = half * n_kv + kv
-        for at in far_peers:
-            peer = 2 * at + near
-            send(block_copy(7, hid_send.at[half], hid_recv, peer, slot, half * n_far + at))
-        send(block_copy(7, hid_send.at[half], hid_recv, partner, slot, half * n_far + far))
+        for peer in [2 * at + near for at in far_peers] + [partner]:
+            kv_copy(7, hid_send.at[half], hid_recv.at[slot], hid_recv_sem.at[slot], peer).start()
     loads[7].wait()
 
     def down(source, block):
@@ -383,7 +344,7 @@
 
     def hid_wait(half, src):
         slot = half * n_kv + src
-        block_copy(7, hid_send.at[half], hid_recv, partner, slot, half * n_far + far).wait_recv()
+        kv_copy(7, hid_recv.at[slot], hid_recv.at[slot], hid_recv_sem.at[slot], partner).wait_recv()
 
     sums = []
     for half in range(2):
@@ -394,16 +355,7 @@
             src = 2 * at + near
             slot = half * n_kv + src
             hid_wait(half, src)
-            send(
-                remote(
-                    hid_recv.at[slot],
-                    hid_recv.at[slot],
-                    kv_send_sem.at[8, half * n_far + at],
-                    kv_recv_sem.at[7, slot],
-                    "kv",
-                    partner,
-                )
-            )
+            kv_copy(10, hid_recv.at[slot], hid_recv.at[slot], hid_recv_sem.at[slot], partner).start()
             total = total + down(src, hid_recv[slot])
         sums.append(total)
     for half in range(2):
@@ -418,19 +370,42 @@
 
             @pl.when(t != tp)
             def _():
-                tp_copy(3, send7.at[t], recv7, t, tp).start()
+                tp_copy(3, 11, send7.at[t], recv7.at[tp], t).start()
 
     recv7[tp] = send7[tp]
-    for off in range(1, n_tp):
-        src = tp_peer(off)
-        tp_copy(3, recv7.at[src], recv7, src, src).wait_recv()
-        tp_copy(3, send7.at[src], recv7, src, tp).wait_send()
+    tp_copy(3, 11, recv7.at[others], recv7.at[others], tp_peer(1)).wait_recv()
     down_out = recv7[0].astype(F32)
     for t in range(1, n_tp):
         down_out = down_out + recv7[t].astype(F32)
     out_ref[...] = (mixed_buf[tp] + down_out).astype(BF16)
-    for copy in sent:
-        copy.wait_send()
+
+    def drain(send_at, buffer, count):
+        block = buffer.at[pl.ds(0, count)]
+        kv_copy(send_at, block, block, sq_recv_sem.at[0], partner).wait_send()
+
+    drain(0, tokbuf, n_tp - 1)
+    drain(1, sq_recv, n_kv - 1)
+    drain(2, mix_recv, n_kv - 1)
+    drain(3, recv4, 2 * (n_tp - 1))
+    drain(4, send2, n_kv)
+    drain(5, send2, n_kv - 2)
+    drain(6, sq5_recv, n_kv - 1)
+    drain(7, send5, n_kv)
+    drain(8, send5, n_kv)
+    drain(9, send5, n_kv - 2)
+    drain(10, send5, n_kv - 2)
+    drain(11, send7, n_tp - 1)
+
+
+def store(tokens_ref, state_ref, tokens_out, state_out, sem):
+    copies = [
+        pltpu.make_async_copy(tokens_ref, tokens_out, sem.at[0]),
+        pltpu.make_async_copy(state_ref, state_out, sem.at[1]),
+    ]
+    for copy in copies:
+        copy.start()
+    for copy in copies:
+        copy.wait()
 
 
 def solution(mesh):
@@ -491,7 +466,7 @@
                 pltpu.VMEM((heads * own, val), BF16),
                 pltpu.VMEM((n_kv, heads * own, val), BF16),
                 pltpu.VMEM((2, rows // 2, feats), BF16),
-                pltpu.VMEM((2, n_tp, rows // 2, feats), BF16),
+                pltpu.VMEM((2 * n_tp, rows // 2, feats), BF16),
                 pltpu.VMEM((n_tp, row_block, feats), F32),
                 pltpu.VMEM((2 * n_kv, rows // 2, chunk), BF16),
                 pltpu.VMEM((n_kv, rows // 2, chunk), BF16),
@@ -504,10 +479,13 @@
                 pltpu.VMEM((n_tp, row_block, feats), BF16),
                 pltpu.VMEM((n_tp, row_block, feats), BF16),
                 pltpu.SemaphoreType.DMA((13,)),
-                pltpu.SemaphoreType.DMA((4, n_tp)),
-                pltpu.SemaphoreType.DMA((4, n_tp)),
-                pltpu.SemaphoreType.DMA((9, 2 * n_kv)),
-                pltpu.SemaphoreType.DMA((9, 2 * n_kv)),
+                pltpu.SemaphoreType.DMA((12,)),
+                pltpu.SemaphoreType.DMA((4,)),
+                pltpu.SemaphoreType.DMA((2,)),
+                pltpu.SemaphoreType.DMA((1,)),
+                pltpu.SemaphoreType.DMA((2, n_kv)),
+                pltpu.SemaphoreType.DMA((4,)),
+                pltpu.SemaphoreType.DMA((2 * n_kv,)),
             ],
             compiler_params=pltpu.CompilerParams(collective_id=0, has_side_effects=True, vmem_limit_bytes=grant),
         )(
@@ -525,7 +503,18 @@
             w_up,
             w_down,
         )
-        return next_tokens, next_state
+        out_shape = (
+            jax.ShapeDtypeStruct(tokens.shape, BF16),
+            jax.ShapeDtypeStruct(recur_state.shape, F32),
+        )
+        return pl.pallas_call(
+            store,
+            out_shape=out_shape,
+            in_specs=[vmem] * 2,
+            out_specs=(hbm, hbm),
+            scratch_shapes=[pltpu.SemaphoreType.DMA((2,))],
+            compiler_params=pltpu.CompilerParams(vmem_limit_bytes=2**20, has_side_effects=True),
+        )(next_tokens, next_state)
 
     in_specs = (
         P("tp", "kv"),

time: 51.1 us -> 48 us (0.939)
  local copies, waits for them, and re-layouts: 2.27 us -> 0 us
  Pallas kernels: 48 us -> 47.2 us
    pallas_call x1, Pallas kernels: 48 us -> 45.5 us  [body(): pl.pallas_call(functools.partial(kernel, n_kv, n_tp), out_shape=(pltpu.VM...]
    unnamed x2 -> x0, local copies, waits for them, and re-layouts: 2.27 us -> none
    pallas_call x0 -> x1, Pallas kernels: none -> 1.69 us  [body(): pl.pallas_call(store, out_shape=out_shape, in_specs=[vmem] * 2, out_specs...]
where the time goes in v1:
time: 48 us; the launch traced here: 47.8 us
  Pallas kernels  47.2 us (98%)
  between operations  0.64 us (1%)
    pallas_call x1, Pallas kernels, body(): pl.pallas_call(functools.partial(kernel, n_kv, n_tp), out_shape=(pltpu.VM...  45.5 us
    pallas_call x1, Pallas kernels, body(): pl.pallas_call(store, out_shape=out_shape, in_specs=[vmem] * 2, out_specs...  1.69 us

profile of v1, /device:TPU:0, one launch (start us, length us, event | category | flops | bytes accessed | tf_op | source)
XLA Modules:
  0.0 47.8 jit_solution(11939108151805430243)
XLA Ops:
  0.6 45.5 %shard_map.140 = (bf16[24,256]{1,0:T(8,128)(2,1)S(1)}, f32[12,4,128,128]{3,2,1,0:T(8,128)S(1)}) custom-call(bf16[24,256]{1,0:T(8,128)(2,1)} %tok_hbm.1, f32[1,256]{1,0:T(1,128)} %bitcast.4, bf16[256,512]{1,0:T(8,128)(2,1)} %wq_hbm.1, bf16[256,512]{1,0:T(8,128)(2,1)} %wf_hbm.1, bf16[256,512]{1,0:T(8,128)(2,1)} %wi_hbm.1, bf16[256,512]{1,0:T(8,128)(2,1)} %wg_hbm.1, ...), custom_call_target="tpu_custom_call" | custom-call | tf_op jit(solution)/shard_map/pallas_call | solution.py:440
  46.1 1.7 %shard_map.141 = (bf16[24,256]{1,0:T(8,128)(2,1)}, f32[12,4,128,128]{3,2,1,0:T(8,128)}) custom-call(bf16[24,256]{1,0:T(8,128)(2,1)S(1)} %get-tuple-element.4.tokens_ref, f32[12,4,128,128]{3,2,1,0:T(8,128)S(1)} %get-tuple-element.5.state_ref), custom_call_target="tpu_custom_call" | custom-call | tf_op jit(solution)/shard_map/pallas_call | solution.py:510
